TPU v7x, 32 devices: a whole 2x2x4 slice. The times are simulated.
32 devices in a mesh: ep: 8 (over z, y), tp: 4 (over x, core).
Axes of the slice: x: 2, y: 2, z: 4, core: 2. Of those that a mesh axis runs over, the one named last changes fastest.
Arguments:
- resid: bfloat16 [256, 2048], P('ep'), may hold values from -6 to 6
- mix_gain: bfloat16 [2048], replicated, may hold values from 0.099609375 to 1.8984375
- proj_x: bfloat16 [2048, 512], P(None, 'tp'), may hold values from -0.125 to 0.125
- proj_z: bfloat16 [2048, 512], P(None, 'tp'), may hold values from -0.125 to 0.125
- proj_b: bfloat16 [2048, 512], P(None, 'tp'), may hold values from -0.125 to 0.125
- proj_c: bfloat16 [2048, 512], P(None, 'tp'), may hold values from -0.125 to 0.125
- proj_step: bfloat16 [2048, 8], replicated, may hold values from -0.125 to 0.125
- step_bias: float32 [8], P('tp'), may hold values from -5 to -1
- decay_rate: float32 [8], P('tp'), may hold values from 1 to 16
- conv_taps: bfloat16 [3, 4, 512], P(None, None, 'tp'), may hold values from -3 to 3
- conv_state: bfloat16 [256, 3, 3, 512], P('ep', None, None, 'tp'), may hold values from -6 to 6
- scan_state: float32 [256, 8, 64, 128], P('ep', 'tp'), may hold values from -2.5 to 2.5
- inner_gain: bfloat16 [512], P('tp'), may hold values from 0.099609375 to 1.8984375
- proj_out: bfloat16 [512, 2048], P('tp'), may hold values from -0.25 to 0.25
- post_gain: bfloat16 [2048], replicated, may hold values from 0.099609375 to 1.8984375
- ffn_gain: bfloat16 [2048], replicated, may hold values from 0.099609375 to 1.8984375
- group_router: bfloat16 [2048, 2], replicated, may hold values from -0.125 to 0.125
- expert_router: bfloat16 [2048, 8], replicated, may hold values from -0.125 to 0.125
- route_experts: int32 [256, 4], P('ep'), may hold values from 0 to 7, as said below
- expert_gate: bfloat16 [8, 2048, 1024], P('ep', None, 'tp'), may hold values from -0.125 to 0.125
- expert_up: bfloat16 [8, 2048, 1024], P('ep', None, 'tp'), may hold values from -0.125 to 0.125
- expert_down: bfloat16 [8, 1024, 2048], P('ep', 'tp')
- dense_switch: bfloat16 [2048], replicated, may hold values from -0.125 to 0.125
- dense_gate: bfloat16 [2048, 2048], P('ep', 'tp'), may hold values from -0.125 to 0.125
- dense_up: bfloat16 [2048, 2048], P('ep', 'tp'), may hold values from -0.125 to 0.125
- dense_down: bfloat16 [2048, 2048], P('ep', 'tp')
- out_gain: bfloat16 [2048], P('tp'), may hold values from 0.099609375 to 1.8984375
Outputs:
- layer_out: bfloat16 [256, 2048], P('ep', 'tp')
- new_state: float32 [256, 8, 64, 128], P('ep', 'tp')
- new_conv: bfloat16 [256, 3, 3, 512], P('ep', None, None, 'tp')
Inputs may be any that keep to these rules, and one draw needn't show every extreme that they name: `route_experts`: each row names 4 different experts, all from one group of 4 consecutive expert numbers. Within each aligned block of 32 rows (the rows of one index of ep) no expert is named more than 32 times, and one expert, the same in every block, is named exactly 32 times in every block.
All inputs are finite; a program needn't handle non-finite values.
Results may differ from a plain program's by a relative error of at most 0.019.
Values may be sent and summed in bfloat16 or wider, within the bound.
A program may use at most 64 MiB of HBM per device.

v0:
```python
import jax
import jax.numpy as jnp
from jax import lax
from jax.sharding import PartitionSpec as P

norm_eps = 1e-06


def scaled_rows(values, gain):
    values = values.astype(jnp.float32)
    mean_square = jnp.mean(values * values, axis=-1, keepdims=True)
    return values * lax.rsqrt(mean_square + norm_eps) * gain.astype(jnp.float32)


def softmax_plain(logits):
    weights = jnp.exp(logits)
    return weights / jnp.sum(weights, axis=-1, keepdims=True)


def on_device(
    resid,
    mix_gain,
    proj_x,
    proj_z,
    proj_b,
    proj_c,
    proj_step,
    step_bias,
    decay_rate,
    conv_taps,
    conv_state,
    scan_state,
    inner_gain,
    proj_out,
    post_gain,
    ffn_gain,
    group_router,
    expert_router,
    route_experts,
    expert_gate,
    expert_up,
    expert_down,
    dense_switch,
    dense_gate,
    dense_up,
    dense_down,
    out_gain,
):
    tp_index = lax.axis_index("tp")
    seqs = resid.shape[0]
    width = resid.shape[1]
    quarter = width // lax.axis_size("tp")
    heads_here = scan_state.shape[1]
    head_dim = scan_state.shape[2]
    state_dim = scan_state.shape[3]
    channels = conv_state.shape[3]
    repeat = heads_here // (channels // state_dim)
    normed = scaled_rows(resid, mix_gain).astype(jnp.bfloat16)
    fresh = jnp.stack(
        [
            jnp.dot(normed, proj_x, preferred_element_type=jnp.float32),
            jnp.dot(normed, proj_b, preferred_element_type=jnp.float32),
            jnp.dot(normed, proj_c, preferred_element_type=jnp.float32),
        ],
        axis=1,
    ).astype(jnp.bfloat16)
    gate_z = jnp.dot(normed, proj_z, preferred_element_type=jnp.float32)
    step_all = jnp.dot(normed, proj_step, preferred_element_type=jnp.float32)
    step_raw = lax.dynamic_slice_in_dim(step_all, tp_index * heads_here, heads_here, 1)
    history = jnp.concatenate([conv_state, fresh[:, :, None, :]], axis=2)
    activated = jax.nn.silu(
        jnp.sum(history.astype(jnp.float32) * conv_taps.astype(jnp.float32)[None], axis=2)
    )
    xs_heads = activated[:, 0].reshape(seqs, heads_here, head_dim)
    b_heads = jnp.repeat(activated[:, 1].reshape(seqs, -1, state_dim), repeat, axis=1)
    c_heads = jnp.repeat(activated[:, 2].reshape(seqs, -1, state_dim), repeat, axis=1)
    step = jax.nn.softplus(step_raw + step_bias)
    keep = jnp.exp(-decay_rate * step)
    driven = step[:, :, None] * xs_heads
    new_state = keep[:, :, None, None] * scan_state + driven[:, :, :, None] * b_heads[:, :, None, :]
    read = jnp.sum(new_state * c_heads[:, :, None, :], axis=3).reshape(seqs, channels)
    gated = (read * jax.nn.silu(gate_z) * inner_gain.astype(jnp.float32)).astype(jnp.bfloat16)
    mixed = lax.psum(
        jnp.dot(gated, proj_out, preferred_element_type=jnp.float32).astype(jnp.bfloat16), "tp"
    ).astype(jnp.float32)
    stream = (resid.astype(jnp.float32) + scaled_rows(mixed, post_gain)).astype(jnp.bfloat16)
    feed = scaled_rows(stream, ffn_gain).astype(jnp.bfloat16)
    feed_quarter = lax.dynamic_slice_in_dim(feed, tp_index * quarter, quarter, 1)
    expert_count = expert_router.shape[1]
    group_size = expert_count // group_router.shape[1]
    pick_count = route_experts.shape[1]
    group_prob = softmax_plain(jnp.dot(feed, group_router, preferred_element_type=jnp.float32))
    expert_logits = jnp.dot(feed, expert_router, preferred_element_type=jnp.float32)
    matches = route_experts[:, :, None] == jnp.arange(expert_count, dtype=jnp.int32)[None, None, :]
    pick_logits = jnp.sum(jnp.where(matches, expert_logits[:, None, :], 0.0), axis=2)
    chosen_group = route_experts[:, 0] // group_size
    group_ids = jnp.arange(group_router.shape[1], dtype=jnp.int32)
    group_weight = jnp.sum(
        jnp.where(chosen_group[:, None] == group_ids[None, :], group_prob, 0.0), axis=1
    )
    pick_weight = softmax_plain(pick_logits) * group_weight[:, None]
    capacity = 2 * seqs * pick_count // expert_count
    flat_picks = route_experts.reshape(-1)
    one_hot = (flat_picks[:, None] == jnp.arange(expert_count, dtype=jnp.int32)[None, :]).astype(
        jnp.int32
    )
    slot = jnp.sum((jnp.cumsum(one_hot, axis=0) - one_hot) * one_hot, axis=1)
    target = flat_picks * capacity + slot
    repeated = jnp.repeat(feed, pick_count, axis=0)
    outgoing = jnp.zeros((expert_count * capacity, width), jnp.bfloat16).at[target].set(repeated)
    outgoing = outgoing.reshape(expert_count, capacity, width)
    arrived = lax.all_to_all(outgoing, "ep", split_axis=0, concat_axis=0, tiled=True)
    sources = arrived.shape[0]
    items = arrived.shape[1]
    rows = arrived.reshape(sources * items, width)
    gate_value = jnp.dot(rows, expert_gate[0], preferred_element_type=jnp.float32)
    up_value = jnp.dot(rows, expert_up[0], preferred_element_type=jnp.float32)
    hidden = (jax.nn.silu(gate_value) * up_value).astype(jnp.bfloat16)
    result = jnp.dot(hidden, expert_down[0], preferred_element_type=jnp.float32).reshape(
        sources, items, width
    )
    summed = lax.psum_scatter(result.astype(jnp.bfloat16), "tp", scatter_dimension=2, tiled=True)
    returned = lax.all_to_all(summed, "ep", split_axis=0, concat_axis=0, tiled=True)
    fetched = returned.reshape(expert_count * capacity, quarter)[target].reshape(
        seqs, pick_count, quarter
    )
    routed = jnp.sum(fetched.astype(jnp.float32) * pick_weight[:, :, None], axis=1)
    gate_piece = jnp.einsum(
        "sd,cd->sc",
        feed_quarter,
        lax.all_gather(dense_gate, "ep", axis=0, tiled=True),
        preferred_element_type=jnp.float32,
    )
    up_piece = jnp.einsum(
        "sd,cd->sc",
        feed_quarter,
        lax.all_gather(dense_up, "ep", axis=0, tiled=True),
        preferred_element_type=jnp.float32,
    )
    gate_sum = gate_piece
    up_sum = up_piece
    gate_sum, up_sum = (
        lax.psum(gate_sum.astype(jnp.bfloat16), "tp").astype(jnp.float32),
        lax.psum(up_sum.astype(jnp.bfloat16), "tp").astype(jnp.float32),
    )
    dense_hidden = (jax.nn.silu(gate_sum) * up_sum).astype(jnp.bfloat16)
    dense_out = jnp.dot(
        dense_hidden,
        lax.all_gather(dense_down, "ep", axis=0, tiled=True),
        preferred_element_type=jnp.float32,
    )
    switch = jax.nn.sigmoid(jnp.dot(feed, dense_switch, preferred_element_type=jnp.float32))
    combined = routed + switch[:, None] * dense_out
    total_square = lax.psum(jnp.sum(combined * combined, axis=1), "tp")
    scale = lax.rsqrt(total_square / width + norm_eps)
    stream_part = lax.dynamic_slice_in_dim(stream, tp_index * quarter, quarter, 1).astype(
        jnp.float32
    )
    layer_out = (stream_part + combined * scale[:, None] * out_gain.astype(jnp.float32)).astype(
        jnp.bfloat16
    )
    new_conv = history[:, :, 1:, :]
    return (layer_out, new_state, new_conv)


def solution(mesh):
    placed = (
        P("ep", None),
        P(),
        P(None, "tp"),
        P(None, "tp"),
        P(None, "tp"),
        P(None, "tp"),
        P(),
        P("tp"),
        P("tp"),
        P(None, None, "tp"),
        P("ep", None, None, "tp"),
        P("ep", "tp", None, None),
        P("tp"),
        P("tp", None),
        P(),
        P(),
        P(),
        P(),
        P("ep", None),
        P("ep", None, "tp"),
        P("ep", None, "tp"),
        P("ep", "tp", None),
        P(),
        P("ep", "tp"),
        P("ep", "tp"),
        P("ep", "tp"),
        P("tp"),
    )
    return jax.shard_map(
        on_device,
        mesh=mesh,
        in_specs=placed,
        out_specs=(P("ep", "tp"), P("ep", "tp", None, None), P("ep", None, None, "tp")),
        check_vma=False,
    )
```

profile of v0, /device:TPU:0, one launch (start us, length us, event | category | flops | bytes accessed | tf_op | source)
XLA Modules:
  0.0 219.6 jit_solution(17043526989973223200)
XLA Ops:
  9.0 1.1 fusion.24
  10.1 1.4 fusion.2
  11.4 1.4 fusion.3
  12.8 1.4 fusion.4
  14.2 0.9 multiply_reduce_fusion.2
  15.3 1.0 fusion.48
  16.7 2.1 multiply_reduce_fusion
  18.9 2.3 %convolution_convert_fusion.3 = bf16[32,2048]{1,0:T(8,128)(2,1)} fusion(bf16[128,2048]{1,0:T(8,128)(2,1)} %param.40, f32[32,128]{1,0:T(8,128)S(1)} %reshape.185, f32[128]{0:T(128)S(1)} %convert_element_type.95, bf16[2048,128]{1,0:T(8,128)(2,1)} %param.30, bf16[32,2048]{1,0:T(8,128)(2,1)S(1)} %copy-done.1, f32[2048]{0:T(1024)S(1)} %convert_element_type.91, ...), kind=kOutput, calls=%fused_computation.5 | convolution fusion | flops 33910784 | bytes 1335936 | tf_op jit(solution)/shard_map/dot_general | solution.py:84
  22.8 33.1 %all-reduce.4.cloned.1.call-done = bf16[32,2048]{1,0:T(8,128)(2,1)} async-done(((bf16[32,2048]{1,0:T(8,128)(2,1)}), bf16[32,2048]{1,0:T(8,128)(2,1)}) %all-reduce.4.cloned.1.call-update) | async-done | bytes 131088 | tf_op jit(solution)/shard_map/psum | solution.py:83
  55.9 1.0 fusion.15
  57.0 1.2 fusion.17
  58.5 0.9 reshape.203
  59.4 2.2 %scatter_custom_fusion = bf16[256,2048]{1,0:T(8,128)(2,1)S(1)} fusion(s32[128]{0:T(128)S(1)} %fusion.39, bf16[128,2048]{1,0:T(8,128)(2,1)} %reshape.203, bf16[]{:T(256)} %constant.57.clone.1), kind=kCustom, calls=%fused_computation.28 | custom fusion | bytes 1049088 | tf_op jit(solution)/shard_map/scatter | solution.py:110
  61.7 36.1 %all_to_all.10 = bf16[8,32,2048]{2,1,0:T(8,128)(2,1)S(1)} all-to-all(bf16[8,32,2048]{2,1,0:T(8,128)(2,1)S(1)} %bitcast.63), channel_id=1, replica_groups=mesh['ep'=8,'tp'=4] {'ep'}, dimensions={0} | all-to-all | bytes 2097152 | tf_op jit(solution)/shard_map/all_to_all | solution.py:112
  98.7 1.4 convolution_convert_fusion
  102.6 3.1 %convolution_convert_fusion.1 = bf16[32,2048]{1,0:T(8,128)(2,1)} fusion(bf16[2048,512]{1,0:T(8,128)(2,1)} %all-gather.6.cloned.1.call-done, bf16[32,2048]{1,0:T(8,128)(2,1)S(1)} %fusion.19, s32[]{:T(128)S(6)} %select_n.38), kind=kOutput, calls=%fused_computation.3 | convolution fusion | flops 67174400 | bytes 2260996 | tf_op jit(solution)/shard_map/sd,cd->sc/dot_general | solution.py:134
  105.7 17.5 %reduce-scatter.2.cloned.1.call-done = bf16[8,32,512]{2,1,0:T(8,128)(2,1)} async-done(((bf16[8,32,2048]{2,1,0:T(8,128)(2,1)}), bf16[8,32,512]{2,1,0:T(8,128)(2,1)}) %reduce-scatter.2.cloned.1.call-update) | async-done | bytes 262160 | tf_op jit(solution)/shard_map/reduce_scatter | solution.py:122
  123.2 5.5 %all-to-all-start.1 = ((bf16[8,32,512]{2,1,0:T(8,128)(2,1)}), bf16[8,32,512]{2,1,0:T(8,128)(2,1)S(1)}, u32[]{:S(2)}, u32[]{:S(2)}) async-start(bf16[8,32,512]{2,1,0:T(8,128)(2,1)} %reduce-scatter.2.cloned.1.call-done), calls=%async_computation.2 | async-start | bytes 524288 | tf_op jit(solution)/shard_map/all_to_all | solution.py:123
  128.8 24.4 %all-gather.4.cloned.1.call-done = bf16[2048,512]{1,0:T(8,128)(2,1)} async-done(((bf16[256,512]{1,0:T(8,128)(2,1)}), bf16[2048,512]{1,0:T(8,128)(2,1)}) %all-gather.4.cloned.1.call-update) | async-done | bytes 2097168 | tf_op jit(solution)/shard_map/all_gather | solution.py:131
  153.2 3.0 %convolution_convert_fusion.2 = bf16[32,2048]{1,0:T(8,128)(2,1)} fusion(bf16[2048,512]{1,0:T(8,128)(2,1)} %all-gather.4.cloned.1.call-done, bf16[32,2048]{1,0:T(8,128)(2,1)S(1)} %fusion.19, s32[]{:T(128)S(6)} %select_n.38), kind=kOutput, calls=%fused_computation.4 | convolution fusion | flops 67174400 | bytes 2260996 | tf_op jit(solution)/shard_map/sd,cd->sc/dot_general | solution.py:128
  156.3 0.8 gather_fusion
  157.5 46.1 %all-gather.8.cloned.1.call-done = bf16[2048,512]{1,0:T(8,128)(2,1)} async-done(((bf16[256,512]{1,0:T(8,128)(2,1)}), bf16[2048,512]{1,0:T(8,128)(2,1)}) %all-gather.8.cloned.1.call-update) | async-done | bytes 2097168 | tf_op jit(solution)/shard_map/all_gather | solution.py:149
  203.6 2.3 %multiply_reduce_fusion.3 = (f32[32]{0:T(128)S(1)}, f32[32,512]{1,0:T(8,128)S(1)}) fusion(f32[32,512]{1,0:T(8,128)S(1)} %multiply_reduce_fusion.1, bf16[2048,512]{1,0:T(8,128)(2,1)} %all-gather.8.cloned.1.call-done, bf16[32,2048]{1,0:T(8,128)(2,1)} %get-tuple-element.3, bf16[32,2048]{1,0:T(8,128)(2,1)} %get-tuple-element.4, f32[32]{0:T(128)S(1)} %fusion.8), kind=kOutput, calls=%fused_computation.58 | convolution fusion | flops 67698656 | bytes 2490624 | tf_op jit(solution)/shard_map/dot_general | solution.py:147
  205.9 5.7 %psum.31 = f32[32]{0:T(128)S(1)} all-reduce(f32[32]{0:T(128)S(1)} %get-tuple-element.18), channel_id=1, replica_groups=mesh['ep'=8,'tp'=4] {'tp'}, use_global_device_ids=true, to_apply=%region_18.19 | all-reduce | flops 32 | bytes 256 | tf_op jit(solution)/shard_map/psum | solution.py:154
  (94 shorter events, 7.8 us)
Async XLA Ops:
  8.0 90.7 %copy-start = (bf16[1,256,2048]{2,1,0:T(8,128)(2,1)S(1)}, bf16[1,256,2048]{2,1,0:T(8,128)(2,1)}, u32[]{:S(2)}) copy-start(bf16[1,256,2048]{2,1,0:T(8,128)(2,1)} %param.48) | copy-start | bytes 3145732
  8.0 7.3 %copy-start.1 = (bf16[32,2048]{1,0:T(8,128)(2,1)S(1)}, bf16[32,2048]{1,0:T(8,128)(2,1)}, u32[]{:S(2)}) copy-start(bf16[32,2048]{1,0:T(8,128)(2,1)} %param.27) | copy-start | bytes 393220
  8.0 6.2 %copy-start.9 = (bf16[3,4,128]{2,1,0:T(4,128)(2,1)S(1)}, bf16[3,4,128]{2,1,0:T(4,128)(2,1)}, u32[]{:S(2)}) copy-start(bf16[3,4,128]{2,1,0:T(4,128)(2,1)} %param.36) | copy-start | bytes 9220
  8.0 8.2 %copy-start.14 = (f32[2]{0:T(128)S(1)}, f32[2]{0:T(128)}, u32[]{:S(2)}) copy-start(f32[2]{0:T(128)} %param.35) | copy-start | bytes 28
  8.0 8.2 %copy-start.11 = (f32[2]{0:T(128)S(1)}, f32[2]{0:T(128)}, u32[]{:S(2)}) copy-start(f32[2]{0:T(128)} %param.34) | copy-start | bytes 28
  8.1 8.6 %copy-start.2 = (f32[32,2,64,128]{3,2,1,0:T(8,128)S(1)}, f32[32,2,64,128]{3,2,1,0:T(8,128)}, u32[]{:S(2)}) copy-start(f32[32,2,64,128]{3,2,1,0:T(8,128)} %param.38) | copy-start | bytes 6291460
  8.1 47.9 %all-reduce.4.cloned.1.call-start = ((), (), s32[]{:S(2)}) async-start(), calls=%async_computation.3 | async-start | bytes 262144 | tf_op jit(solution)/shard_map/psum | solution.py:83
  16.7 2.2 %copy-start.15 = (bf16[128]{0:T(256)(128)(2,1)S(1)}, bf16[128]{0:T(256)(128)(2,1)}, u32[]{:S(2)}) copy-start(bf16[128]{0:T(256)(128)(2,1)} %param.39) | copy-start | bytes 772
  16.7 5.2 %copy-start.5 = (s32[32,4]{0,1:T(4,128)S(1)}, s32[32,4]{0,1:T(4,128)}, u32[]{:S(2)}) copy-start(s32[32,4]{0,1:T(4,128)} %param.45) | copy-start | bytes 1540
  16.7 5.3 %copy-start.6 = (bf16[2048]{0:T(1024)(128)(2,1)S(1)}, bf16[2048]{0:T(1024)(128)(2,1)}, u32[]{:S(2)}) copy-start(bf16[2048]{0:T(1024)(128)(2,1)} %param.41) | copy-start | bytes 12292
  16.7 5.3 %copy-start.7 = (bf16[2048]{0:T(1024)(128)(2,1)S(1)}, bf16[2048]{0:T(1024)(128)(2,1)}, u32[]{:S(2)}) copy-start(bf16[2048]{0:T(1024)(128)(2,1)} %param.42) | copy-start | bytes 12292
  21.3 81.3 %all-gather.6.cloned.1.call-start = ((), (), s32[]{:S(2)}) async-start(), calls=%async_computation.6 | async-start | bytes 2359296 | tf_op jit(solution)/shard_map/all_gather | solution.py:137
  21.9 101.4 %reduce-scatter.2.cloned.1.call-start = ((), (), s32[]{:S(2)}) async-start(), calls=%async_computation.4 | async-start | bytes 1310720 | tf_op jit(solution)/shard_map/reduce_scatter | solution.py:122
  58.5 39.2 %copy-start.3 = (bf16[1,2048,256]{2,1,0:T(8,128)(2,1)S(1)}, bf16[1,2048,256]{2,1,0:T(8,128)(2,1)}, u32[]{:S(2)}) copy-start(bf16[1,2048,256]{2,1,0:T(8,128)(2,1)} %param.46) | copy-start | bytes 3145732
  61.6 36.5 %copy-start.12 = (bf16[1,2048,256]{2,1,0:T(8,128)(2,1)S(1)}, bf16[1,2048,256]{2,1,0:T(8,128)(2,1)}, u32[]{:S(2)}) copy-start(bf16[1,2048,256]{2,1,0:T(8,128)(2,1)} %param.47) | copy-start | bytes 3145732
  98.6 2.7 %copy-start.8 = (bf16[2048]{0:T(1024)(128)(2,1)S(1)}, bf16[2048]{0:T(1024)(128)(2,1)}, u32[]{:S(2)}) copy-start(bf16[2048]{0:T(1024)(128)(2,1)} %param.49) | copy-start | bytes 12292
  98.6 2.7 %copy-start.10 = (bf16[512]{0:T(512)(128)(2,1)S(1)}, bf16[512]{0:T(512)(128)(2,1)}, u32[]{:S(2)}) copy-start(bf16[512]{0:T(512)(128)(2,1)} %param.53) | copy-start | bytes 3076
  98.7 3.4 %copy-start.4 = (bf16[2048,8]{0,1:T(8,128)(2,1)S(1)}, bf16[2048,8]{0,1:T(8,128)(2,1)}, u32[]{:S(2)}) copy-start(bf16[2048,8]{0,1:T(8,128)(2,1)} %param.44) | copy-start | bytes 98308
  98.7 3.6 %copy-start.13 = (bf16[2048,2]{0,1:T(2,128)(2,1)S(1)}, bf16[2048,2]{0,1:T(2,128)(2,1)}, u32[]{:S(2)}) copy-start(bf16[2048,2]{0,1:T(2,128)(2,1)} %param.43) | copy-start | bytes 24580
  100.2 53.1 %all-gather.4.cloned.1.call-start = ((), (), s32[]{:S(2)}) async-start(), calls=%async_computation.5 | async-start | bytes 2359296 | tf_op jit(solution)/shard_map/all_gather | solution.py:131
  100.7 102.8 %all-gather.8.cloned.1.call-start = ((), (), s32[]{:S(2)}) async-start(), calls=%async_computation.7 | async-start | bytes 2359296 | tf_op jit(solution)/shard_map/all_gather | solution.py:149
  123.2 33.1 %all-to-all-start.1 = ((bf16[8,32,512]{2,1,0:T(8,128)(2,1)}), bf16[8,32,512]{2,1,0:T(8,128)(2,1)S(1)}, u32[]{:S(2)}, u32[]{:S(2)}) async-start(bf16[8,32,512]{2,1,0:T(8,128)(2,1)} %reduce-scatter.2.cloned.1.call-done), calls=%async_computation.2 | async-start | bytes 524288 | tf_op jit(solution)/shard_map/all_to_all | solution.py:123
  128.8 74.8 %all-reduce.6.cloned.1.call-start = ((), (), s32[]{:S(2)}) async-start(), calls=%async_computation.8 | async-start | bytes 524288 | tf_op jit(solution)/shard_map/psum | solution.py:144
Sparse Core Ops, SparseCore 0:
  21.4 34.4 all-reduce.3
  100.3 22.9 reduce-scatter.1
  156.3 31.6 all-reduce.5
Sparse Core Ops, SparseCore 1:
  23.9 59.7 all-gather.5
  102.8 50.4 all-gather.3
  155.2 48.3 all-gather.7
where the time goes:
time: 220 us
  waiting for transfers between devices  123 us (56%)
  blocking collectives  41.7 us (19%)
  matrix products  18.6 us (8%)
  between operations  15.9 us (7%)
  other arithmetic  8.99 us (4%)
  local copies, waits for them, and re-layouts  5.86 us (3%)
  starting transfers between devices  5.78 us (3%)
    all_gather x1, waiting for transfers between devices, on_device(): lax.all_gather(dense_down, 'ep', axis=0, tiled=True)  46.1 us
    all_to_all x1, blocking collectives, on_device(): lax.all_to_all(outgoing, 'ep', split_axis=0, concat_axis=0, tiled=True)  36.1 us
    psum x1, waiting for transfers between devices, on_device(): lax.psum(jnp.dot(gated, proj_out, preferred_element_type=jnp.float32).ast...  33.1 us
    all_gather x1, waiting for transfers between devices, on_device(): lax.all_gather(dense_gate, 'ep', axis=0, tiled=True)  24.4 us
    reduce_scatter x1, waiting for transfers between devices, on_device(): lax.psum_scatter(result.astype(jnp.bfloat16), 'tp', scatter_dimension=2,...  17.5 us
    psum x1, blocking collectives, on_device(): total_square = lax.psum(jnp.sum(combined * combined, axis=1), 'tp')  5.67 us
    all_to_all x1, starting transfers between devices, on_device(): lax.all_to_all(summed, 'ep', split_axis=0, concat_axis=0, tiled=True)  5.53 us
  transfers between devices with their start and end apart: 7, of which 4 were waited for; matrix products, arithmetic and copies ran while one was open for 8% of the time, Pallas kernels for 0%

commit v1 on v0

--- a/solution.py
+++ b/solution.py
@@ -125,12 +125,29 @@
         seqs, pick_count, quarter
     )
     routed = jnp.sum(fetched.astype(jnp.float32) * pick_weight[:, :, None], axis=1)
-    gate_piece = jnp.einsum(
-        "sd,cd->sc",
-        feed_quarter,
-        lax.all_gather(dense_gate, "ep", axis=0, tiled=True),
-        preferred_element_type=jnp.float32,
-    )
+    q_next = lax.axis_index("ep")
+    value_now = lax.axis_size("ep")
+    small, tile_out, w_next = (value_now, q_next, dense_gate.shape[0])
+    built = carry_in = dense_gate
+    ready, response = ([], [])
+    for pp in range(small // 2 + 1):
+        carry = jnp.einsum("sd,cd->sc", feed_quarter, built, preferred_element_type=jnp.float32)
+        ready.append(carry)
+        if 0 < pp < small - small // 2:
+            upper = jnp.einsum(
+                "sd,cd->sc", feed_quarter, carry_in, preferred_element_type=jnp.float32
+            )
+            response.append(upper)
+        pile = []
+        for b in range(small):
+            pile.append((b, (b + 1) % small))
+        built = lax.ppermute(built, "ep", pile)
+        log = []
+        for b in range(small):
+            log.append((b, (b - 1) % small))
+        carry_in = lax.ppermute(carry_in, "ep", log)
+    before = jnp.concatenate([*ready[::-1], *response], 1)
+    gate_piece = jnp.roll(before, (tile_out - small // 2) * ready[0].shape[1], 1)
     up_piece = jnp.einsum(
         "sd,cd->sc",
         feed_quarter,

time: 220 us -> 232 us (1.055)
  starting transfers between devices: 5.78 us -> 19.1 us
  waiting for transfers between devices: 123 us -> 129 us
  blocking collectives: 41.7 us -> 35.9 us
    ppermute x0 -> x7, waiting for transfers between devices: none -> 43.3 us  [the longest x4 39.7 us: on_device(): built = lax.ppermute(built, 'ep', pile)]
    all_gather x1 -> x0, waiting for transfers between devices: 24.4 us -> none  [on_device(): lax.all_gather(dense_gate, 'ep', axis=0, tiled=True)]
    reduce_scatter x1, waiting for transfers between devices: 17.5 us -> 0.01 us  [on_device(): lax.psum_scatter(result.astype(jnp.bfloat16), 'tp', scatter_dimension=2,...]
    ppermute x0 -> x7, starting transfers between devices: none -> 15.5 us  [the longest x3 8.34 us: on_device(): carry_in = lax.ppermute(carry_in, 'ep', log)]
    all_to_all x1, blocking collectives: 36.1 us -> 30.2 us  [on_device(): lax.all_to_all(outgoing, 'ep', split_axis=0, concat_axis=0, tiled=True)]
    all_gather x1, waiting for transfers between devices: 0.01 us -> 4.8 us  [on_device(): lax.all_gather(dense_up, 'ep', axis=0, tiled=True)]
  transfers between devices with their start and end apart: 7 -> 13, of which waited for: 4 -> 10; matrix products, arithmetic and copies ran while one was open for 8% -> 4% of each run, Pallas kernels for 0% -> 0%
where the time goes in v1:
time: 232 us
  waiting for transfers between devices  129 us (56%)
  blocking collectives  35.9 us (15%)
  starting transfers between devices  19.1 us (8%)
  matrix products  16.9 us (7%)
  between operations  15.7 us (7%)
  other arithmetic  8.98 us (4%)
  local copies, waits for them, and re-layouts  6.56 us (3%)
    all_gather x1, waiting for transfers between devices, on_device(): lax.all_gather(dense_down, 'ep', axis=0, tiled=True)  45.9 us
    ppermute x4, waiting for transfers between devices, on_device(): built = lax.ppermute(built, 'ep', pile)  39.7 us
    psum x1, waiting for transfers between devices, on_device(): lax.psum(jnp.dot(gated, proj_out, preferred_element_type=jnp.float32).ast...  33.8 us
    all_to_all x1, blocking collectives, on_device(): lax.all_to_all(outgoing, 'ep', split_axis=0, concat_axis=0, tiled=True)  30.2 us
    ppermute x3, starting transfers between devices, on_device(): carry_in = lax.ppermute(carry_in, 'ep', log)  8.34 us
    ppermute x4, starting transfers between devices, on_device(): built = lax.ppermute(built, 'ep', pile)  7.18 us
    psum x1, blocking collectives, on_device(): total_square = lax.psum(jnp.sum(combined * combined, axis=1), 'tp')  5.67 us
    all_gather x1, waiting for transfers between devices, on_device(): lax.all_gather(dense_up, 'ep', axis=0, tiled=True)  4.8 us
  transfers between devices with their start and end apart: 13, of which 10 were waited for; matrix products, arithmetic and copies ran while one was open for 4% of the time, Pallas kernels for 0%

profile of v1, /device:TPU:0, one launch (start us, length us, event | category | flops | bytes accessed | tf_op | source)
XLA Modules:
  0.0 231.7 jit_solution(6356211131729690227)
XLA Ops:
  10.1 1.4 fusion.2
  11.4 1.4 fusion.3
  16.7 2.1 multiply_reduce_fusion
  18.9 2.3 %convolution_convert_fusion.2 = bf16[32,2048]{1,0:T(8,128)(2,1)} fusion(bf16[128,2048]{1,0:T(8,128)(2,1)} %param.40, f32[32,128]{1,0:T(8,128)S(1)} %reshape.185, f32[128]{0:T(128)S(1)} %convert_element_type.95, bf16[2048,128]{1,0:T(8,128)(2,1)} %param.30, bf16[32,2048]{1,0:T(8,128)(2,1)S(1)} %copy-done.1, f32[2048]{0:T(1024)S(1)} %convert_element_type.91, ...), kind=kOutput, calls=%fused_computation.4 | convolution fusion | flops 33910784 | bytes 1335936 | tf_op jit(solution)/shard_map/dot_general | solution.py:84
  22.2 33.8 %all-reduce.4.cloned.1.call-done = bf16[32,2048]{1,0:T(8,128)(2,1)} async-done(((bf16[32,2048]{1,0:T(8,128)(2,1)}), bf16[32,2048]{1,0:T(8,128)(2,1)}) %all-reduce.4.cloned.1.call-update) | async-done | bytes 131088 | tf_op jit(solution)/shard_map/psum | solution.py:83
  59.5 2.2 scatter_custom_fusion
  61.7 30.2 %all_to_all.10 = bf16[8,32,2048]{2,1,0:T(8,128)(2,1)S(1)} all-to-all(bf16[8,32,2048]{2,1,0:T(8,128)(2,1)S(1)} %bitcast.70), channel_id=1, replica_groups=mesh['ep'=8,'tp'=4] {'ep'}, dimensions={0} | all-to-all | bytes 2097152 | tf_op jit(solution)/shard_map/all_to_all | solution.py:112
  92.9 1.4 convolution_convert_fusion
  95.0 1.5 collective-permute-start
  96.4 3.3 %collective-permute-start.4 = (bf16[256,512]{1,0:T(8,128)(2,1)S(1)}, bf16[256,512]{1,0:T(8,128)(2,1)S(1)}, u32[]{:S(2)}, u32[]{:S(2)}) collective-permute-start(bf16[256,512]{1,0:T(8,128)(2,1)S(1)} %copy-done.4), channel_id=1, source_target_pairs={{0,28},{4,0},{8,4},{12,8},{16,12},{20,16},{24,20},{28,24},{1,29},{... | collective-permute-start | bytes 786440 | tf_op jit(solution)/shard_map/ppermute | solution.py:148
  99.8 9.6 %collective-permute-done = bf16[256,512]{1,0:T(8,128)(2,1)S(1)} collective-permute-done((bf16[256,512]{1,0:T(8,128)(2,1)S(1)}, bf16[256,512]{1,0:T(8,128)(2,1)S(1)}, u32[]{:S(2)}, u32[]{:S(2)}) %collective-permute-start) | collective-permute-done | bytes 262176 | tf_op jit(solution)/shard_map/ppermute | solution.py:144
  109.4 2.5 %collective-permute-start.1 = (bf16[256,512]{1,0:T(8,128)(2,1)S(1)}, bf16[256,512]{1,0:T(8,128)(2,1)S(1)}, u32[]{:S(2)}, u32[]{:S(2)}) collective-permute-start(bf16[256,512]{1,0:T(8,128)(2,1)S(1)} %collective-permute-done), channel_id=1, source_target_pairs={{0,4},{4,8},{8,12},{12,16},{16,20},{20,24},{24,28},{28,0},{1,5},{5... | collective-permute-start | bytes 786440 | tf_op jit(solution)/shard_map/ppermute | solution.py:144
  112.7 10.1 %collective-permute-done.1 = bf16[256,512]{1,0:T(8,128)(2,1)S(1)} collective-permute-done((bf16[256,512]{1,0:T(8,128)(2,1)S(1)}, bf16[256,512]{1,0:T(8,128)(2,1)S(1)}, u32[]{:S(2)}, u32[]{:S(2)}) %collective-permute-start.1) | collective-permute-done | bytes 262176 | tf_op jit(solution)/shard_map/ppermute | solution.py:144
  123.1 4.8 %collective-permute-start.5 = (bf16[256,512]{1,0:T(8,128)(2,1)S(1)}, bf16[256,512]{1,0:T(8,128)(2,1)S(1)}, u32[]{:S(2)}, u32[]{:S(2)}) collective-permute-start(bf16[256,512]{1,0:T(8,128)(2,1)S(1)} %collective-permute-done.4), channel_id=1, source_target_pairs={{0,28},{4,0},{8,4},{12,8},{16,12},{20,16},{24,20},{28,24},{1,29},{... | collective-permute-start | bytes 786440 | tf_op jit(solution)/shard_map/ppermute | solution.py:148
  127.8 10.0 %collective-permute-done.2 = bf16[256,512]{1,0:T(8,128)(2,1)S(1)} collective-permute-done((bf16[256,512]{1,0:T(8,128)(2,1)S(1)}, bf16[256,512]{1,0:T(8,128)(2,1)S(1)}, u32[]{:S(2)}, u32[]{:S(2)}) %collective-permute-start.2) | collective-permute-done | bytes 262176 | tf_op jit(solution)/shard_map/ppermute | solution.py:144
  137.9 3.2 %collective-permute-start.3 = (bf16[256,512]{1,0:T(8,128)(2,1)S(1)}, bf16[256,512]{1,0:T(8,128)(2,1)S(1)}, u32[]{:S(2)}, u32[]{:S(2)}) collective-permute-start(bf16[256,512]{1,0:T(8,128)(2,1)S(1)} %collective-permute-done.2), channel_id=1, source_target_pairs={{0,4},{4,8},{8,12},{12,16},{16,20},{20,24},{24,28},{28,0},{1,5},{5... | collective-permute-start | bytes 786440 | tf_op jit(solution)/shard_map/ppermute | solution.py:144
  142.8 9.9 %collective-permute-done.3 = bf16[256,512]{1,0:T(8,128)(2,1)S(1)} collective-permute-done((bf16[256,512]{1,0:T(8,128)(2,1)S(1)}, bf16[256,512]{1,0:T(8,128)(2,1)S(1)}, u32[]{:S(2)}, u32[]{:S(2)}) %collective-permute-start.3) | collective-permute-done | bytes 262176 | tf_op jit(solution)/shard_map/ppermute | solution.py:144
  154.0 2.3 %collective-permute-done.6 = bf16[256,512]{1,0:T(8,128)(2,1)S(1)} collective-permute-done((bf16[256,512]{1,0:T(8,128)(2,1)S(1)}, bf16[256,512]{1,0:T(8,128)(2,1)S(1)}, u32[]{:S(2)}, u32[]{:S(2)}) %collective-permute-start.6) | collective-permute-done | bytes 262176 | tf_op jit(solution)/shard_map/ppermute | solution.py:148
  157.3 3.4 %all-to-all-start.1 = ((bf16[8,32,512]{2,1,0:T(8,128)(2,1)}), bf16[8,32,512]{2,1,0:T(8,128)(2,1)S(1)}, u32[]{:S(2)}, u32[]{:S(2)}) async-start(bf16[8,32,512]{2,1,0:T(8,128)(2,1)} %reduce-scatter.2.cloned.1.call-done), calls=%async_computation.2 | async-start | bytes 524288 | tf_op jit(solution)/shard_map/all_to_all | solution.py:123
  160.7 4.8 %all-gather.3.cloned.1.call-done = bf16[2048,512]{1,0:T(8,128)(2,1)} async-done(((bf16[256,512]{1,0:T(8,128)(2,1)}), bf16[2048,512]{1,0:T(8,128)(2,1)}) %all-gather.3.cloned.1.call-update) | async-done | bytes 2097168 | tf_op jit(solution)/shard_map/all_gather | solution.py:154
  165.5 2.9 %convolution_convert_fusion.1 = bf16[32,2048]{1,0:T(8,128)(2,1)} fusion(bf16[2048,512]{1,0:T(8,128)(2,1)} %all-gather.3.cloned.1.call-done, bf16[32,2048]{1,0:T(8,128)(2,1)S(1)} %fusion.19, s32[]{:T(128)S(6)} %select_n.51), kind=kOutput, calls=%fused_computation.3 | convolution fusion | flops 67174400 | bytes 2260996 | tf_op jit(solution)/shard_map/sd,cd->sc/dot_general | solution.py:151
  170.0 45.9 %all-gather.5.cloned.1.call-done = bf16[2048,512]{1,0:T(8,128)(2,1)} async-done(((bf16[256,512]{1,0:T(8,128)(2,1)}), bf16[2048,512]{1,0:T(8,128)(2,1)}) %all-gather.5.cloned.1.call-update) | async-done | bytes 2097168 | tf_op jit(solution)/shard_map/all_gather | solution.py:166
  215.9 2.3 multiply_reduce_fusion.3
  218.2 5.7 %psum.31 = f32[32]{0:T(128)S(1)} all-reduce(f32[32]{0:T(128)S(1)} %get-tuple-element.34), channel_id=1, replica_groups=mesh['ep'=8,'tp'=4] {'tp'}, use_global_device_ids=true, to_apply=%region_18.19 | all-reduce | flops 32 | bytes 256 | tf_op jit(solution)/shard_map/psum | solution.py:171
  (123 shorter events, 19.0 us)
Async XLA Ops:
  8.0 84.9 %copy-start = (bf16[1,256,2048]{2,1,0:T(8,128)(2,1)S(1)}, bf16[1,256,2048]{2,1,0:T(8,128)(2,1)}, u32[]{:S(2)}) copy-start(bf16[1,256,2048]{2,1,0:T(8,128)(2,1)} %param.48) | copy-start | bytes 3145732
  8.0 7.3 %copy-start.1 = (bf16[32,2048]{1,0:T(8,128)(2,1)S(1)}, bf16[32,2048]{1,0:T(8,128)(2,1)}, u32[]{:S(2)}) copy-start(bf16[32,2048]{1,0:T(8,128)(2,1)} %param.27) | copy-start | bytes 393220
  8.0 8.2 %copy-start.15 = (f32[2]{0:T(128)S(1)}, f32[2]{0:T(128)}, u32[]{:S(2)}) copy-start(f32[2]{0:T(128)} %param.35) | copy-start | bytes 28
  8.0 8.2 %copy-start.12 = (f32[2]{0:T(128)S(1)}, f32[2]{0:T(128)}, u32[]{:S(2)}) copy-start(f32[2]{0:T(128)} %param.34) | copy-start | bytes 28
  8.1 8.6 %copy-start.2 = (f32[32,2,64,128]{3,2,1,0:T(8,128)S(1)}, f32[32,2,64,128]{3,2,1,0:T(8,128)}, u32[]{:S(2)}) copy-start(f32[32,2,64,128]{3,2,1,0:T(8,128)} %param.38) | copy-start | bytes 6291460
  8.1 47.9 %all-reduce.4.cloned.1.call-start = ((), (), s32[]{:S(2)}) async-start(), calls=%async_computation.3 | async-start | bytes 262144 | tf_op jit(solution)/shard_map/psum | solution.py:83
  21.3 136.0 %reduce-scatter.2.cloned.1.call-start = ((), (), s32[]{:S(2)}) async-start(), calls=%async_computation.4 | async-start | bytes 1310720 | tf_op jit(solution)/shard_map/reduce_scatter | solution.py:122
  58.6 33.3 %copy-start.3 = (bf16[1,2048,256]{2,1,0:T(8,128)(2,1)S(1)}, bf16[1,2048,256]{2,1,0:T(8,128)(2,1)}, u32[]{:S(2)}) copy-start(bf16[1,2048,256]{2,1,0:T(8,128)(2,1)} %param.46) | copy-start | bytes 3145732
  61.7 30.6 %copy-start.13 = (bf16[1,2048,256]{2,1,0:T(8,128)(2,1)S(1)}, bf16[1,2048,256]{2,1,0:T(8,128)(2,1)}, u32[]{:S(2)}) copy-start(bf16[1,2048,256]{2,1,0:T(8,128)(2,1)} %param.47) | copy-start | bytes 3145732
  92.8 19.1 %copy-start.9 = (bf16[2048]{0:T(1024)(128)(2,1)S(1)}, bf16[2048]{0:T(1024)(128)(2,1)}, u32[]{:S(2)}) copy-start(bf16[2048]{0:T(1024)(128)(2,1)} %param.49) | copy-start | bytes 12292
  92.8 19.1 %copy-start.11 = (bf16[512]{0:T(512)(128)(2,1)S(1)}, bf16[512]{0:T(512)(128)(2,1)}, u32[]{:S(2)}) copy-start(bf16[512]{0:T(512)(128)(2,1)} %param.53) | copy-start | bytes 3076
  92.8 19.8 %copy-start.5 = (bf16[2048,8]{0,1:T(8,128)(2,1)S(1)}, bf16[2048,8]{0,1:T(8,128)(2,1)}, u32[]{:S(2)}) copy-start(bf16[2048,8]{0,1:T(8,128)(2,1)} %param.44) | copy-start | bytes 98308
  92.8 30.0 %copy-start.14 = (bf16[2048,2]{0,1:T(2,128)(2,1)S(1)}, bf16[2048,2]{0,1:T(2,128)(2,1)}, u32[]{:S(2)}) copy-start(bf16[2048,2]{0,1:T(2,128)(2,1)} %param.43) | copy-start | bytes 24580
  94.3 71.2 %all-gather.3.cloned.1.call-start = ((), (), s32[]{:S(2)}) async-start(), calls=%async_computation.5 | async-start | bytes 2359296 | tf_op jit(solution)/shard_map/all_gather | solution.py:154
  94.9 121.0 %all-gather.5.cloned.1.call-start = ((), (), s32[]{:S(2)}) async-start(), calls=%async_computation.6 | async-start | bytes 2359296 | tf_op jit(solution)/shard_map/all_gather | solution.py:166
  95.0 14.5 %collective-permute-start = (bf16[256,512]{1,0:T(8,128)(2,1)S(1)}, bf16[256,512]{1,0:T(8,128)(2,1)S(1)}, u32[]{:S(2)}, u32[]{:S(2)}) collective-permute-start(bf16[256,512]{1,0:T(8,128)(2,1)S(1)} %copy-done.4), channel_id=1, source_target_pairs={{0,4},{4,8},{8,12},{12,16},{16,20},{20,24},{24,28},{28,0},{1,5},{5... | collective-permute-start | bytes 786440 | tf_op jit(solution)/shard_map/ppermute | solution.py:144
  96.4 26.6 %collective-permute-start.4 = (bf16[256,512]{1,0:T(8,128)(2,1)S(1)}, bf16[256,512]{1,0:T(8,128)(2,1)S(1)}, u32[]{:S(2)}, u32[]{:S(2)}) collective-permute-start(bf16[256,512]{1,0:T(8,128)(2,1)S(1)} %copy-done.4), channel_id=1, source_target_pairs={{0,28},{4,0},{8,4},{12,8},{16,12},{20,16},{24,20},{28,24},{1,29},{... | collective-permute-start | bytes 786440 | tf_op jit(solution)/shard_map/ppermute | solution.py:148
  109.4 13.4 %collective-permute-start.1 = (bf16[256,512]{1,0:T(8,128)(2,1)S(1)}, bf16[256,512]{1,0:T(8,128)(2,1)S(1)}, u32[]{:S(2)}, u32[]{:S(2)}) collective-permute-start(bf16[256,512]{1,0:T(8,128)(2,1)S(1)} %collective-permute-done), channel_id=1, source_target_pairs={{0,4},{4,8},{8,12},{12,16},{16,20},{20,24},{24,28},{28,0},{1,5},{5... | collective-permute-start | bytes 786440 | tf_op jit(solution)/shard_map/ppermute | solution.py:144
  122.8 15.0 %collective-permute-start.2 = (bf16[256,512]{1,0:T(8,128)(2,1)S(1)}, bf16[256,512]{1,0:T(8,128)(2,1)S(1)}, u32[]{:S(2)}, u32[]{:S(2)}) collective-permute-start(bf16[256,512]{1,0:T(8,128)(2,1)S(1)} %collective-permute-done.1), channel_id=1, source_target_pairs={{0,4},{4,8},{8,12},{12,16},{16,20},{20,24},{24,28},{28,0},{1,5},{5... | collective-permute-start | bytes 786440 | tf_op jit(solution)/shard_map/ppermute | solution.py:144
  123.1 19.5 %collective-permute-start.5 = (bf16[256,512]{1,0:T(8,128)(2,1)S(1)}, bf16[256,512]{1,0:T(8,128)(2,1)S(1)}, u32[]{:S(2)}, u32[]{:S(2)}) collective-permute-start(bf16[256,512]{1,0:T(8,128)(2,1)S(1)} %collective-permute-done.4), channel_id=1, source_target_pairs={{0,28},{4,0},{8,4},{12,8},{16,12},{20,16},{24,20},{28,24},{1,29},{... | collective-permute-start | bytes 786440 | tf_op jit(solution)/shard_map/ppermute | solution.py:148
  137.9 14.8 %collective-permute-start.3 = (bf16[256,512]{1,0:T(8,128)(2,1)S(1)}, bf16[256,512]{1,0:T(8,128)(2,1)S(1)}, u32[]{:S(2)}, u32[]{:S(2)}) collective-permute-start(bf16[256,512]{1,0:T(8,128)(2,1)S(1)} %collective-permute-done.2), channel_id=1, source_target_pairs={{0,4},{4,8},{8,12},{12,16},{16,20},{20,24},{24,28},{28,0},{1,5},{5... | collective-permute-start | bytes 786440 | tf_op jit(solution)/shard_map/ppermute | solution.py:144
  142.5 13.8 %collective-permute-start.6 = (bf16[256,512]{1,0:T(8,128)(2,1)S(1)}, bf16[256,512]{1,0:T(8,128)(2,1)S(1)}, u32[]{:S(2)}, u32[]{:S(2)}) collective-permute-start(bf16[256,512]{1,0:T(8,128)(2,1)S(1)} %collective-permute-done.5), channel_id=1, source_target_pairs={{0,28},{4,0},{8,4},{12,8},{16,12},{20,16},{24,20},{28,24},{1,29},{... | collective-permute-start | bytes 786440 | tf_op jit(solution)/shard_map/ppermute | solution.py:148
  157.3 11.6 %all-to-all-start.1 = ((bf16[8,32,512]{2,1,0:T(8,128)(2,1)}), bf16[8,32,512]{2,1,0:T(8,128)(2,1)S(1)}, u32[]{:S(2)}, u32[]{:S(2)}) async-start(bf16[8,32,512]{2,1,0:T(8,128)(2,1)} %reduce-scatter.2.cloned.1.call-done), calls=%async_computation.2 | async-start | bytes 524288 | tf_op jit(solution)/shard_map/all_to_all | solution.py:123
  160.7 55.2 %all-reduce.6.cloned.1.call-start = ((), (), s32[]{:S(2)}) async-start(), calls=%async_computation.7 | async-start | bytes 524288 | tf_op jit(solution)/shard_map/psum | solution.py:161
  (6 other events, 26.2 us)
Sparse Core Ops, SparseCore 0:
  21.4 34.5 all-reduce.3
  94.4 23.0 reduce-scatter.1
  168.6 31.7 all-reduce.5
Sparse Core Ops, SparseCore 1:
  96.9 68.6 all-gather.2
  167.5 48.3 all-gather.4
